TPU v7x, 256 devices: a whole 4x4x8 slice. The times are simulated.
256 devices in a mesh: ep: 64 (over z, y, core), tp: 4 (over x).
Axes of the slice: x: 4, y: 4, z: 8, core: 2. Of those that a mesh axis runs over, the one named last changes fastest.
Arguments:
- queries: bfloat16 [12288, 8, 128], P('ep', 'tp'), may hold values from -140 to 140
- keys: bfloat16 [12288, 4, 128], P('ep', 'tp'), may hold values from -6 to 6
- values: bfloat16 [12288, 4, 128], P('ep', 'tp'), may hold values from -6 to 6
- mix_scale: float32 [8], P('tp'), may hold values from 0.3 to 0.8
- head_gain: float32 [128], replicated, may hold values from 0.1 to 1.9
- out_weight: bfloat16 [8, 128, 2048], P('tp'), may hold values from -0.1875 to 0.1875
- moe_input: bfloat16 [24576, 2048], P(('ep', 'tp')), may hold values from -6 to 6
- norm_gain: float32 [2048], replicated, may hold values from 0.1 to 1.9
- routes: int32 [24576, 2], P(('ep', 'tp')), may hold values from 0 to 63, all different within a row; in each aligned block of 96 rows (0 to 95, 96 to 191, ...) at most 4 rows name the same one
- route_weights: float32 [24576, 2], P(('ep', 'tp')), may hold values from 0.2 to 1
- gate_weight: bfloat16 [64, 2048, 3584], P('ep', None, 'tp'), may hold values from -0.125 to 0.125
- up_weight: bfloat16 [64, 2048, 3584], P('ep', None, 'tp'), may hold values from -0.125 to 0.125
- down_weight: bfloat16 [64, 3584, 2048], P('ep', 'tp'), may hold values from -0.09375 to 0.09375
Outputs:
- attn_out: bfloat16 [12288, 2048], P(('ep', 'tp'))
- moe_out: bfloat16 [24576, 2048], P(('ep', 'tp'))
Inputs may be any that keep to these rules, and one draw needn't show every extreme that they name: `routes`: the 2 experts of a row differ. In each aligned block of 96 rows (the rows of one device) no expert is named by more than 4 rows, and in some blocks an expert is named by exactly 4 rows.
All inputs are finite; a program needn't handle non-finite values.
Results may differ from a plain program's by a relative error of at most 0.014.
Values may be sent and summed in bfloat16 or wider, within the bound.
A program may use at most 128 MiB of HBM per device.

v0:
```python
import math
import jax
import jax.numpy as jnp
from jax import lax
from jax.sharding import Mesh
from jax.sharding import PartitionSpec as P

EP = ("ep_0", "ep_1", "ep_2")
EP_TP = ("ep_0", "ep_1", "ep_2", "tp")
NEG_LARGE = -1e30


def joined_along(tiles, dim):
    tiles = jnp.moveaxis(tiles, 0, dim)
    lengths = tiles.shape
    return tiles.reshape(*lengths[:dim], lengths[dim] * lengths[dim + 1], *lengths[dim + 2 :])


def gather_in_order(value, axes, order):
    tiles = value[None]
    for k in order:
        tiles = lax.all_gather(tiles, axes[k], axis=0, tiled=True)
    current = [lax.axis_size(axes[k]) for k in reversed(order)]
    tiles = tiles.reshape(*current, *value.shape)
    turned = sorted(range(len(order)), key=lambda place: order[len(order) - 1 - place])
    return tiles.transpose(*turned, *range(len(order), tiles.ndim)).reshape(-1, *value.shape)


def gathered_by_axis(value, axes, order, dim):
    return joined_along(gather_in_order(value, axes, order), dim)


def split_up(value, dim, peers):
    before, after = (value.shape[:dim], value.shape[dim + 1 :])
    return jnp.moveaxis(value.reshape(*before, peers, -1, *after), dim, 0)


def summed_on_arrival(value, axis, dim):
    peers = lax.axis_size(axis)
    tiles = lax.all_to_all(split_up(value, dim, peers), axis, 0, 0, tiled=True)
    return jnp.sum(tiles.astype(jnp.float32), axis=0)


def attend_update(running, query_set, positions, key_block, value_block, key_anchor, scaling):
    row_peak, totals, numerator = running
    span = key_block.shape[0]
    scores = (
        jnp.einsum("tkgmd,skmd->kgmts", query_set, key_block, preferred_element_type=jnp.float32)
        * scaling
    )
    visible = (key_anchor + jnp.arange(span, dtype=jnp.int32))[None, :] <= positions[:, None]
    scores = jnp.where(visible, scores, NEG_LARGE)
    new_peak = jnp.maximum(row_peak, jnp.max(scores, axis=-1))
    weights = jnp.where(visible, jnp.exp(scores - new_peak[..., None]), 0.0)
    factor = jnp.exp(row_peak - new_peak)
    totals = totals * factor + jnp.sum(weights, axis=-1)
    numerator = numerator * factor[..., None] + jnp.einsum(
        "rnouf,frj->rnouj",
        weights.astype(jnp.bfloat16),
        value_block,
        preferred_element_type=jnp.float32,
    )
    return (new_peak, totals, numerator)


def body(
    queries,
    keys,
    values,
    mix_scale,
    head_gain,
    out_weight,
    moe_input,
    norm_gain,
    routes,
    route_weights,
    gate_weight,
    up_weight,
    down_weight,
):
    rows_here = queries.shape[0]
    key_heads = keys.shape[1]
    head_count = queries.shape[1]
    group_size = head_count // key_heads
    head_dim = queries.shape[2] // 2
    value_dim = values.shape[2]
    ep_size = lax.axis_size(EP)
    own_start = lax.axis_index(EP) * rows_here
    grouped = queries.reshape(rows_here, key_heads, group_size, 2, head_dim)
    own_positions = own_start + jnp.arange(rows_here, dtype=jnp.int32)
    query_sets = ((grouped, own_positions),)
    scaling = 1.0 / math.sqrt(head_dim)

    def empty_state(row_total):
        return (
            jnp.full((key_heads, group_size, 2, row_total), NEG_LARGE, jnp.float32),
            jnp.zeros((key_heads, group_size, 2, row_total), jnp.float32),
            jnp.zeros((key_heads, group_size, 2, row_total, value_dim), jnp.float32),
        )

    initial = tuple((empty_state(entry[0].shape[0]) for entry in query_sets))
    key_rows = gathered_by_axis(keys, EP, (1, 0, 2), 0)
    value_rows = gathered_by_axis(values, EP, (1, 0, 2), 0)
    length = key_rows.shape[0]
    span = length
    while span > 1024 and span % 2 == 0:
        span = span // 2
    key_rows = key_rows.reshape(length, key_heads, 2, head_dim)

    def sweep(step_id, states):
        anchor = step_id * span
        key_block = lax.dynamic_slice_in_dim(key_rows, step_id * span, span, 0)
        value_block = lax.dynamic_slice_in_dim(value_rows, step_id * span, span, 0)
        updated = []
        for (query_set, positions), status in zip(query_sets, states):

            def advance(current):
                return attend_update(
                    current, query_set, positions, key_block, value_block, anchor, scaling
                )

            def unchanged(current):
                return current

            updated.append(lax.cond(anchor <= positions[-1], advance, unchanged, status))
        return tuple(updated)

    folded = lax.fori_loop(0, length // span, sweep, initial)
    mixing = mix_scale.reshape(key_heads, group_size, 1, 1)
    outputs = []
    for status in folded:
        row_peak, totals, numerator = status
        blended = numerator[:, :, 0] / totals[:, :, 0, :, None] - mixing * (
            numerator[:, :, 1] / totals[:, :, 1, :, None]
        )
        normed = (
            blended
            * lax.rsqrt(jnp.mean(blended * blended, axis=-1, keepdims=True) + 1e-05)
            * head_gain
        )
        outputs.append(
            jnp.transpose(normed.astype(jnp.bfloat16), (2, 0, 1, 3)).reshape(
                -1, head_count * value_dim
            )
        )
    head_flat = outputs[0]
    weight_flat = out_weight.reshape(head_count * value_dim, -1)
    widened = moe_input.astype(jnp.float32)
    normed_in = (
        widened * lax.rsqrt(jnp.mean(widened * widened, axis=-1, keepdims=True) + 1e-06) * norm_gain
    ).astype(jnp.bfloat16)
    tok_count = moe_input.shape[0]
    top_count = routes.shape[1]
    experts = ep_size * gate_weight.shape[0]
    capacity = max(2, 3 * top_count * tok_count // (2 * experts))
    flattened = routes.reshape(-1)
    one_hot = (flattened[:, None] == jnp.arange(experts, dtype=jnp.int32)[None, :]).astype(
        jnp.int32
    )
    before = jnp.cumsum(one_hot, axis=0) - one_hot
    ranking = jnp.sum(before * one_hot, axis=1)
    slot_ids = (flattened * capacity + ranking).reshape(tok_count, top_count)
    slot_total = experts * capacity
    dispatch = jnp.any(
        jnp.arange(slot_total, dtype=jnp.int32)[:, None, None] == slot_ids[None], axis=2
    ).astype(jnp.bfloat16)
    outbound = jnp.dot(dispatch, normed_in, preferred_element_type=jnp.float32).astype(jnp.bfloat16)
    received = lax.all_to_all(outbound, EP, split_axis=0, concat_axis=0, tiled=True)
    inputs = lax.all_gather(received, "tp", axis=0, tiled=True)
    gate_proj = jnp.dot(inputs, gate_weight[0], preferred_element_type=jnp.float32)
    up_proj = jnp.dot(inputs, up_weight[0], preferred_element_type=jnp.float32)
    hidden_all = (jax.nn.silu(gate_proj) * up_proj).astype(jnp.bfloat16)
    attn_out = summed_on_arrival(
        jnp.dot(head_flat, weight_flat, preferred_element_type=jnp.float32).astype(jnp.bfloat16),
        "tp",
        0,
    ).astype(jnp.bfloat16)
    expert_out = summed_on_arrival(
        jnp.dot(hidden_all, down_weight[0], preferred_element_type=jnp.float32).astype(
            jnp.bfloat16
        ),
        "tp",
        0,
    ).astype(jnp.bfloat16)
    returned_rows = lax.all_to_all(expert_out, EP, split_axis=0, concat_axis=0, tiled=True)
    picked = jnp.take(returned_rows, slot_ids, axis=0)
    moe_out = jnp.sum(route_weights[:, :, None] * picked.astype(jnp.float32), axis=1).astype(
        jnp.bfloat16
    )
    return (attn_out, moe_out)


def solution(mesh):
    split = Mesh(mesh.devices.reshape(8, 4, 2, mesh.shape["tp"]), ("ep_0", "ep_1", "ep_2", "tp"))
    placed = (
        P(EP, "tp", None),
        P(EP, "tp", None),
        P(EP, "tp", None),
        P("tp"),
        P(),
        P("tp", None, None),
        P(EP_TP, None),
        P(),
        P(EP_TP, None),
        P(EP_TP, None),
        P(EP, None, "tp"),
        P(EP, None, "tp"),
        P(EP, "tp", None),
    )
    return jax.shard_map(
        body,
        mesh=split,
        in_specs=placed,
        out_specs=(P(EP_TP, None), P(EP_TP, None)),
        check_vma=False,
    )
```

profile of v0, /device:TPU:1, one launch (start us, length us, event | category | flops | bytes accessed | tf_op | source)
XLA Modules:
  0.0 368.3 jit_solution(15211746906782629320)
XLA Ops:
  7.2 12.6 %all-gather = bf16[768,1,128]{2,0,1:T(8,128)(2,1)} all-gather(bf16[192,1,128]{2,0,1:T(8,128)(2,1)} %param.18), channel_id=2, replica_groups=mesh['ep_0'=8,'ep_1'=4,'ep_2'=2,'tp'=4] {'ep_1'}, dimensions={0}, use_global_device_ids=true | all-gather | bytes 245760 | tf_op jit(solution)/shard_map/all_gather | solution.py:22
  19.9 10.2 %all-gather.1 = bf16[768,1,128]{2,0,1:T(8,128)(2,1)} all-gather(bf16[192,1,128]{2,0,1:T(8,128)(2,1)} %param.19), channel_id=3, replica_groups=mesh['ep_0'=8,'ep_1'=4,'ep_2'=2,'tp'=4] {'ep_1'}, dimensions={0}, use_global_device_ids=true | all-gather | bytes 245760 | tf_op jit(solution)/shard_map/all_gather | solution.py:22
  30.2 0.8 copy.86
  31.0 0.1 eq.35
  31.1 0.6 reduce-window.6
  31.7 0.2 slice_reduce_fusion
  32.1 0.1 reduce_sum.76
  32.3 0.7 compare_and_fusion
  33.1 1.2 fusion.22
  34.3 1.5 convolution_convert_fusion.1
  35.8 0.4 all_to_all.23
  36.3 47.2 %all_to_all.34 = bf16[64,4,2048]{2,1,0:T(4,128)(2,1)S(1)} all-to-all(bf16[64,4,2048]{2,1,0:T(4,128)(2,1)S(1)} %all_to_all.23), channel_id=1, replica_groups=mesh['ep_0'=8,'ep_1'=4,'ep_2'=2,'tp'=4] {'ep_0','ep_1','ep_2'}, dimensions={0} | all-to-all | bytes 2097152 | tf_op jit(solution)/shard_map/all_to_all | solution.py:168
  83.5 1.1 all_to_all.25
  84.7 0.5 all-gather.10.cloned.1.call-update
  85.2 23.4 %all-gather.12.cloned.1.call-done = bf16[32,192,1,128]{3,1,2,0:T(8,128)(2,1)} async-done(((bf16[4,192,1,128]{3,1,2,0:T(8,128)(2,1)}), bf16[32,192,1,128]{3,1,2,0:T(8,128)(2,1)}) %all-gather.12.cloned.1.call-update) | async-done | bytes 1572880 | tf_op jit(solution)/shard_map/all_gather | solution.py:22
  108.7 54.8 %all-gather.16.cloned.1.call-done = bf16[1024,2048]{1,0:T(8,128)(2,1)} async-done(((bf16[256,2048]{1,0:T(8,128)(2,1)}), bf16[1024,2048]{1,0:T(8,128)(2,1)}) %all-gather.16.cloned.1.call-update) | async-done | bytes 4194320 | tf_op jit(solution)/shard_map/all_gather | solution.py:169
  163.5 7.5 %fusion.16 = f32[1024,896]{1,0:T(8,128)S(1)} fusion(bf16[1024,2048]{1,0:T(8,128)(2,1)} %all-gather.16.cloned.1.call-done, bf16[1,2048,896]{2,1,0:T(8,128)(2,1)} %param.28), kind=kOutput, calls=%fused_computation.26 | convolution fusion | flops 3758096384 | bytes 11534336 | tf_op jit(solution)/shard_map/dot_general | solution.py:171
  171.0 4.7 %multiply_convert_fusion = bf16[1024,896]{1,0:T(8,128)(2,1)S(1)} fusion(f32[1024,896]{1,0:T(8,128)S(1)} %fusion.16, bf16[1024,2048]{1,0:T(8,128)(2,1)S(1)} %copy-done.5, bf16[1,2048,896]{2,1,0:T(8,128)(2,1)S(1)} %copy-done.6), kind=kOutput, calls=%fused_computation.30 | convolution fusion | flops 3763601408 | bytes 13369344 | tf_op jit(solution)/shard_map/dot_general | solution.py:170
  175.8 6.1 %convolution_convert_fusion = bf16[1024,2048]{1,0:T(8,128)(2,1)} fusion(bf16[1024,896]{1,0:T(8,128)(2,1)S(1)} %multiply_convert_fusion, bf16[1,896,2048]{2,1,0:T(8,128)(2,1)S(1)} %copy-done.7), kind=kOutput, calls=%fused_computation.24 | convolution fusion | flops 3760193536 | bytes 9699328 | tf_op jit(solution)/shard_map/dot_general | solution.py:179
  181.9 5.1 %all-to-all-start.2 = ((bf16[4,256,2048]{2,1,0:T(8,128)(2,1)}), bf16[4,256,2048]{2,1,0:T(8,128)(2,1)}, u32[]{:S(2)}, u32[]{:S(2)}) async-start(bf16[4,256,2048]{2,1,0:T(8,128)(2,1)} %bitcast.121), calls=%async_computation.2 | async-start | bytes 8388608 | tf_op jit(solution)/shard_map/all_to_all | solution.py:40
  187.1 0.1 copy.80
  187.2 11.2 %copy.79 = bf16[8,4,2,192,1,128]{3,2,1,0,5,4:T(2,128)(2,1)} copy(bf16[8,4,2,192,1,128]{5,3,1,0,2,4:T(8,128)(2,1)} %bitcast.122) | data formatting | bytes 6291456 | tf_op jit(solution)/shard_map/transpose | solution.py:26
  198.4 9.9 %reshape_reshape_reshape.3 = bf16[12288,1,2,64]{0,3,2,1:T(8,128)(2,1)} reshape(bf16[8,4,2,192,1,128]{3,2,1,0,5,4:T(2,128)(2,1)} %copy.79) | data formatting | bytes 6291456 | tf_op jit(solution)/shard_map/reshape;reshape;reshape | solution.py:108
  208.4 3.9 %copy.81 = bf16[8,4,2,192,1,128]{5,3,2,1,0,4:T(8,128)(2,1)} copy(bf16[8,4,2,192,1,128]{5,3,1,0,2,4:T(8,128)(2,1)} %bitcast.124) | data formatting | bytes 6291456 | tf_op jit(solution)/shard_map/transpose | solution.py:26
  212.3 24.4 %while.17 = (s32[]{:T(128)}, f32[1,2,2,192]{3,1,2,0:T(2,128)S(1)}, f32[1,2,2,192]{3,1,2,0:T(2,128)S(1)}, f32[1,2,2,192,128]{4,3,2,1,0:T(8,128)S(1)}, s32[192]{0:...) while((s32[]{:T(128)}, f32[1,2,2,192]{3,1,2,0:T(2,128)S(1)}, ...), condition=%wide.region_5.6_spmd, body=%wide.region_0.5_spmd.sunk | while | flops 232147968 | bytes 8857645 | solution.py:128
  212.4 0.6 slice.57
  213.6 4.3 %conditional.2 = ((f32[1,2,2,192]{3,1,2,0:T(2,128)S(1)}, f32[1,2,2,192]{3,1,2,0:T(2,128)S(1)}, f32[1,2,2,192,128]{4,3,2,1,0:T(8,128)S(1)})) conditional(s32[]{:T(128)} %convert_element_type.91, (f32[1,2,2,192]{3,1,2,0:T(2,128)S(1)}, f32[1,2,2,192]{3,1,2,0:T(2,128)S(1)}, f32[1,2,2,192,128]{4,3,2,1,0:T(8,128)S(1)}) %tuple.61, (s32[]{:T(128)}, ...), branch_computations={%region_1.0_spmd, %region_2.4_spmd} | conditional | flops 232147968 | bytes 8857422 | solution.py:125
  213.6 0.1 broadcast_compare_fusion
  213.8 1.6 fusion
  215.4 0.9 fusion.4
  216.3 1.5 fusion.3
  217.9 0.6 slice.57
  219.1 0.6 slice.57
  220.4 0.6 slice.57
  221.7 0.6 slice.57
  222.9 0.6 slice.57
  224.2 0.6 slice.57
  225.4 0.6 slice.57
  226.7 0.6 slice.57
  227.9 0.6 slice.57
  229.2 0.6 slice.57
  230.4 0.6 slice.57
  231.7 0.6 slice.57
  233.0 0.6 slice.57
  234.2 0.6 slice.57
  235.5 0.6 slice.57
  236.7 0.3 multiply_reduce_fusion.1
  237.1 0.1 fusion.32
  237.3 1.3 convolution_convert_fusion.2
  238.6 4.0 %all-to-all-start = ((bf16[4,48,2048]{2,1,0:T(8,128)(2,1)}), bf16[4,48,2048]{2,1,0:T(8,128)(2,1)S(1)}, u32[]{:S(2)}, u32[]{:S(2)}) async-start(bf16[4,48,2048]{2,1,0:T(8,128)(2,1)} %bitcast.30), calls=%async_computation | async-start | bytes 1572864 | tf_op jit(solution)/shard_map/all_to_all | solution.py:40
  242.6 3.1 reduce_sum.78
  245.7 1.2 all_to_all.27
  246.9 6.6 %all-to-all-done = bf16[4,48,2048]{2,1,0:T(8,128)(2,1)S(1)} async-done(((bf16[4,48,2048]{2,1,0:T(8,128)(2,1)}), bf16[4,48,2048]{2,1,0:T(8,128)(2,1)S(1)}, u32[]{:S(2)}, u32[]{:S(2)}) %all-to-all-start) | async-done | bytes 786464 | tf_op jit(solution)/shard_map/all_to_all | solution.py:40
  253.5 74.0 %all-to-all-start.3 = ((bf16[64,4,2048]{2,1,0:T(4,128)(2,1)}), bf16[64,4,2048]{2,1,0:T(4,128)(2,1)S(1)}, u32[]{:S(2)}, u32[]{:S(2)}) async-start(bf16[64,4,2048]{2,1,0:T(4,128)(2,1)} %all_to_all.27), calls=%async_computation.3 | async-start | bytes 2097152 | tf_op jit(solution)/shard_map/all_to_all | solution.py:185
  327.5 0.1 copy.91
  327.6 0.1 reshape.218
  327.7 0.1 copy.90
  327.9 0.1 copy.85
  328.0 0.8 reduce_sum.74
  328.8 26.8 %all-to-all-done.3 = bf16[64,4,2048]{2,1,0:T(4,128)(2,1)S(1)} async-done(((bf16[64,4,2048]{2,1,0:T(4,128)(2,1)}), bf16[64,4,2048]{2,1,0:T(4,128)(2,1)S(1)}, u32[]{:S(2)}, u32[]{:S(2)}) %all-to-all-start.3) | async-done | bytes 1048608 | tf_op jit(solution)/shard_map/all_to_all | solution.py:185
  355.6 0.3 all_to_all.29
  355.9 1.1 gather_fusion
  357.1 0.5 reshape.217
  357.6 4.2 %multiply_reduce_fusion = bf16[96,2048]{1,0:T(8,128)(2,1)} fusion(bf16[96,2,2048]{2,1,0:T(2,128)(2,1)S(1)} %reshape.217, pred[96,2]{1,0:T(8,128)(4,1)S(1)} %copy.90, f32[96,2]{1,0:T(8,128)S(1)} %copy.85), kind=kLoop, calls=%fused_computation.33 | loop fusion | flops 1376256 | bytes 1180608 | tf_op jit(solution)/shard_map/reduce_sum | solution.py:187
  (68 shorter events, 1.1 us)
Async XLA Ops:
  7.2 230.1 %copy-start = (bf16[2,128,2048]{2,1,0:T(8,128)(2,1)S(1)}, bf16[2,128,2048]{2,1,0:T(8,128)(2,1)}, u32[]{:S(2)}) copy-start(bf16[2,128,2048]{2,1,0:T(8,128)(2,1)} %param.22) | copy-start | bytes 3145732
  7.2 77.5 %all-gather.8.cloned.1.call-start = ((), (), s32[]{:S(2)}) async-start(), calls=%async_computation.4 | async-start | bytes 1769472 | tf_op jit(solution)/shard_map/all_gather | solution.py:22
  19.9 88.8 %all-gather.12.cloned.1.call-start = ((), (), s32[]{:S(2)}) async-start(), calls=%async_computation.6 | async-start | bytes 1769472 | tf_op jit(solution)/shard_map/all_gather | solution.py:22
  30.1 133.4 %all-gather.16.cloned.1.call-start = ((), (), s32[]{:S(2)}) async-start(), calls=%async_computation.8 | async-start | bytes 5242880 | tf_op jit(solution)/shard_map/all_gather | solution.py:169
  84.6 102.6 %all-gather.10.cloned.1.call-start = ((), (), s32[]{:S(2)}) async-start(), calls=%async_computation.5 | async-start | bytes 4718592 | tf_op jit(solution)/shard_map/all_gather | solution.py:22
  85.2 123.2 %all-gather.14.cloned.1.call-start = ((), (), s32[]{:S(2)}) async-start(), calls=%async_computation.7 | async-start | bytes 4718592 | tf_op jit(solution)/shard_map/all_gather | solution.py:22
  163.5 7.5 %copy-start.5 = (bf16[1024,2048]{1,0:T(8,128)(2,1)S(1)}, bf16[1024,2048]{1,0:T(8,128)(2,1)}, u32[]{:S(2)}) copy-start(bf16[1024,2048]{1,0:T(8,128)(2,1)} %all-gather.16.cloned.1.call-done) | copy-start | bytes 12582916
  163.5 7.5 %copy-start.6 = (bf16[1,2048,896]{2,1,0:T(8,128)(2,1)S(1)}, bf16[1,2048,896]{2,1,0:T(8,128)(2,1)}, u32[]{:S(2)}) copy-start(bf16[1,2048,896]{2,1,0:T(8,128)(2,1)} %param.27) | copy-start | bytes 11010052
  171.0 4.8 %copy-start.7 = (bf16[1,896,2048]{2,1,0:T(8,128)(2,1)S(1)}, bf16[1,896,2048]{2,1,0:T(8,128)(2,1)}, u32[]{:S(2)}) copy-start(bf16[1,896,2048]{2,1,0:T(8,128)(2,1)} %param.29) | copy-start | bytes 11010052
  181.9 5.2 %copy-start.1 = (bf16[192,2,128]{2,1,0:T(2,128)(2,1)S(1)}, bf16[192,2,128]{2,1,0:T(2,128)(2,1)}, u32[]{:S(2)}) copy-start(bf16[192,2,128]{2,1,0:T(2,128)(2,1)} %param.17) | copy-start | bytes 294916
  181.9 56.7 %all-to-all-start.2 = ((bf16[4,256,2048]{2,1,0:T(8,128)(2,1)}), bf16[4,256,2048]{2,1,0:T(8,128)(2,1)}, u32[]{:S(2)}, u32[]{:S(2)}) async-start(bf16[4,256,2048]{2,1,0:T(8,128)(2,1)} %bitcast.121), calls=%async_computation.2 | async-start | bytes 8388608 | tf_op jit(solution)/shard_map/all_to_all | solution.py:40
  212.3 24.4 %copy-start.4 = (f32[2]{0:T(128)S(1)}, f32[2]{0:T(128)}, u32[]{:S(2)}) copy-start(f32[2]{0:T(128)} %param.20) | copy-start | bytes 28
  212.3 24.7 %copy-start.3 = (f32[128]{0:T(128)S(1)}, f32[128]{0:T(128)}, u32[]{:S(2)}) copy-start(f32[128]{0:T(128)} %param.21) | copy-start | bytes 1540
  238.6 14.9 %all-to-all-start = ((bf16[4,48,2048]{2,1,0:T(8,128)(2,1)}), bf16[4,48,2048]{2,1,0:T(8,128)(2,1)S(1)}, u32[]{:S(2)}, u32[]{:S(2)}) async-start(bf16[4,48,2048]{2,1,0:T(8,128)(2,1)} %bitcast.30), calls=%async_computation | async-start | bytes 1572864 | tf_op jit(solution)/shard_map/all_to_all | solution.py:40
  245.7 82.2 %copy-start.2 = (f32[96,2]{0,1:T(2,128)S(1)}, f32[96,2]{0,1:T(2,128)}, u32[]{:S(2)}) copy-start(f32[96,2]{0,1:T(2,128)} %param.26) | copy-start | bytes 2308
  253.5 102.2 %all-to-all-start.3 = ((bf16[64,4,2048]{2,1,0:T(4,128)(2,1)}), bf16[64,4,2048]{2,1,0:T(4,128)(2,1)S(1)}, u32[]{:S(2)}, u32[]{:S(2)}) async-start(bf16[64,4,2048]{2,1,0:T(4,128)(2,1)} %all_to_all.27), calls=%async_computation.3 | async-start | bytes 2097152 | tf_op jit(solution)/shard_map/all_to_all | solution.py:185
Sparse Core Ops, SparseCore 0:
  20.0 43.5 all-gather.7
  65.3 43.2 all-gather.11
  110.5 52.9 all-gather.15
  165.2 18.7 all-gather.9
  185.6 18.7 all-gather.13
where the time goes:
time: 370 us; the launch traced here: 368 us
  waiting for transfers between devices  112 us (30%)
  starting transfers between devices  83.3 us (23%)
  blocking collectives  70 us (19%)
  local copies, waits for them, and re-layouts  41.2 us (11%)
  matrix products  24.3 us (7%)
  between operations  14.1 us (4%)
  other arithmetic  12.4 us (3%)
  loops' own time  10.7 us (3%)
    all_to_all x1, starting transfers between devices, body(): lax.all_to_all(expert_out, EP, split_axis=0, concat_axis=0, tiled=True)  74 us
    all_gather x1, waiting for transfers between devices, body(): inputs = lax.all_gather(received, 'tp', axis=0, tiled=True)  54.8 us
    all_to_all x1, blocking collectives, body(): lax.all_to_all(outbound, EP, split_axis=0, concat_axis=0, tiled=True)  47.2 us
    all_to_all x1, waiting for transfers between devices, body(): lax.all_to_all(expert_out, EP, split_axis=0, concat_axis=0, tiled=True)  26.8 us
    all_gather x4, waiting for transfers between devices, gather_in_order(): tiles = lax.all_gather(tiles, axes[k], axis=0, tiled=True)  23.5 us
    all_gather x2, blocking collectives, gather_in_order(): tiles = lax.all_gather(tiles, axes[k], axis=0, tiled=True)  22.8 us
    transpose x2, local copies, waits for them, and re-layouts, gather_in_order(): tiles.transpose(*turned, *range(len(order), tiles.ndim))  15.1 us
    another operation x1, loops' own time, body(): folded = lax.fori_loop(0, length // span, sweep, initial)  10.4 us
  transfers between devices with their start and end apart: 8, of which 4 were waited for; matrix products, arithmetic and copies ran while one was open for 19% of the time, Pallas kernels for 0%

commit v1 on v0

--- a/solution.py
+++ b/solution.py
@@ -166,7 +166,9 @@
     ).astype(jnp.bfloat16)
     outbound = jnp.dot(dispatch, normed_in, preferred_element_type=jnp.float32).astype(jnp.bfloat16)
     received = lax.all_to_all(outbound, EP, split_axis=0, concat_axis=0, tiled=True)
-    inputs = lax.all_gather(received, "tp", axis=0, tiled=True)
+    inputs = jnp.concatenate(
+        lax.all_to_all(jnp.stack([received] * lax.axis_size("tp")), "tp", 0, 0), axis=0
+    )
     gate_proj = jnp.dot(inputs, gate_weight[0], preferred_element_type=jnp.float32)
     up_proj = jnp.dot(inputs, up_weight[0], preferred_element_type=jnp.float32)
     hidden_all = (jax.nn.silu(gate_proj) * up_proj).astype(jnp.bfloat16)

time: 370 us -> 349 us (0.943)
  waiting for transfers between devices: 112 us -> 79.8 us
  local copies, waits for them, and re-layouts: 41.2 us -> 45.7 us
    all_gather x1 -> x0, waiting for transfers between devices: 54.8 us -> none  [body(): inputs = lax.all_gather(received, 'tp', axis=0, tiled=True)]
    all_to_all x0 -> x1, waiting for transfers between devices: none -> 31.9 us  [body(): lax.all_to_all(jnp.stack([received] * lax.axis_size('tp')), 'tp', 0, 0)]
    all_gather x4, waiting for transfers between devices: 23.5 us -> 16.3 us  [gather_in_order(): tiles = lax.all_gather(tiles, axes[k], axis=0, tiled=True)]
    all_to_all x0 -> x1, starting transfers between devices: none -> 4.85 us  [body(): lax.all_to_all(jnp.stack([received] * lax.axis_size('tp')), 'tp', 0, 0)]
    another operation x2 -> x4, local copies, waits for them, and re-layouts: 0.19 us -> 4.09 us  [the longest x2 3.9 us: body(): jnp.stack([received] * lax.axis_size('tp'))]
  transfers between devices with their start and end apart: 8 -> 8, of which waited for: 4 -> 4; matrix products, arithmetic and copies ran while one was open for 19% -> 22% of each run, Pallas kernels for 0% -> 0%
where the time goes in v1:
time: 349 us; the launch traced here: 347 us
  starting transfers between devices  86.3 us (25%)
  waiting for transfers between devices  79.8 us (23%)
  blocking collectives  70.1 us (20%)
  local copies, waits for them, and re-layouts  45.7 us (13%)
  matrix products  26.9 us (8%)
  between operations  14.1 us (4%)
  other arithmetic  13.5 us (4%)
  loops' own time  10.9 us (3%)
    all_to_all x1, starting transfers between devices, body(): lax.all_to_all(expert_out, EP, split_axis=0, concat_axis=0, tiled=True)  72.2 us
    all_to_all x1, blocking collectives, body(): lax.all_to_all(outbound, EP, split_axis=0, concat_axis=0, tiled=True)  47.3 us
    all_to_all x1, waiting for transfers between devices, body(): lax.all_to_all(jnp.stack([received] * lax.axis_size('tp')), 'tp', 0, 0)  31.9 us
    all_to_all x1, waiting for transfers between devices, body(): lax.all_to_all(expert_out, EP, split_axis=0, concat_axis=0, tiled=True)  25.7 us
    all_gather x2, blocking collectives, gather_in_order(): tiles = lax.all_gather(tiles, axes[k], axis=0, tiled=True)  22.8 us
    all_gather x4, waiting for transfers between devices, gather_in_order(): tiles = lax.all_gather(tiles, axes[k], axis=0, tiled=True)  16.3 us
    transpose x2, local copies, waits for them, and re-layouts, gather_in_order(): tiles.transpose(*turned, *range(len(order), tiles.ndim))  15.1 us
    another operation x1, loops' own time, body(): folded = lax.fori_loop(0, length // span, sweep, initial)  10.7 us
  transfers between devices with their start and end apart: 8, of which 4 were waited for; matrix products, arithmetic and copies ran while one was open for 22% of the time, Pallas kernels for 0%

profile of v1, /device:TPU:1, one launch (start us, length us, event | category | flops | bytes accessed | tf_op | source)
XLA Modules:
  0.0 347.3 jit_solution(563593959831310710)
XLA Ops:
  7.2 12.6 %all-gather = bf16[768,1,128]{2,0,1:T(8,128)(2,1)} all-gather(bf16[192,1,128]{2,0,1:T(8,128)(2,1)} %param.18), channel_id=2, replica_groups=mesh['ep_0'=8,'ep_1'=4,'ep_2'=2,'tp'=4] {'ep_1'}, dimensions={0}, use_global_device_ids=true | all-gather | bytes 245760 | tf_op jit(solution)/shard_map/all_gather | solution.py:22
  19.9 10.2 %all-gather.1 = bf16[768,1,128]{2,0,1:T(8,128)(2,1)} all-gather(bf16[192,1,128]{2,0,1:T(8,128)(2,1)} %param.19), channel_id=3, replica_groups=mesh['ep_0'=8,'ep_1'=4,'ep_2'=2,'tp'=4] {'ep_1'}, dimensions={0}, use_global_device_ids=true | all-gather | bytes 245760 | tf_op jit(solution)/shard_map/all_gather | solution.py:22
  30.2 0.8 copy.86
  31.0 0.1 eq.35
  31.1 0.6 reduce-window.6
  31.7 0.2 slice_reduce_fusion
  32.1 0.1 reduce_sum.76
  32.3 0.7 compare_and_fusion
  33.1 1.2 fusion.22
  34.3 1.5 convolution_convert_fusion.1
  35.8 0.4 all_to_all.24
  36.3 47.3 %all_to_all.36 = bf16[64,4,2048]{2,1,0:T(4,128)(2,1)} all-to-all(bf16[64,4,2048]{2,1,0:T(4,128)(2,1)S(1)} %all_to_all.24), channel_id=1, replica_groups=mesh['ep_0'=8,'ep_1'=4,'ep_2'=2,'tp'=4] {'ep_0','ep_1','ep_2'}, dimensions={0} | all-to-all | bytes 2097152 | tf_op jit(solution)/shard_map/all_to_all | solution.py:168
  83.6 1.4 stack.4
  85.0 2.5 stack.10
  87.5 4.8 %all-to-all-start.2 = ((bf16[4,256,2048]{2,1,0:T(8,128)(2,1)}), bf16[4,256,2048]{2,1,0:T(8,128)(2,1)}, u32[]{:S(2)}, u32[]{:S(2)}) async-start(bf16[4,256,2048]{2,1,0:T(8,128)(2,1)} %stack.10), calls=%async_computation.2 | async-start | bytes 8388608 | tf_op jit(solution)/shard_map/all_to_all | solution.py:170
  92.4 16.2 %all-gather.11.cloned.1.call-done = bf16[32,192,1,128]{3,1,2,0:T(8,128)(2,1)} async-done(((bf16[4,192,1,128]{3,1,2,0:T(8,128)(2,1)}), bf16[32,192,1,128]{3,1,2,0:T(8,128)(2,1)}) %all-gather.11.cloned.1.call-update) | async-done | bytes 1572880 | tf_op jit(solution)/shard_map/all_gather | solution.py:22
  108.7 31.9 %all-to-all-done.2 = bf16[4,256,2048]{2,1,0:T(8,128)(2,1)} async-done(((bf16[4,256,2048]{2,1,0:T(8,128)(2,1)}), bf16[4,256,2048]{2,1,0:T(8,128)(2,1)}, u32[]{:S(2)}, u32[]{:S(2)}) %all-to-all-start.2) | async-done | bytes 4194336 | tf_op jit(solution)/shard_map/all_to_all | solution.py:170
  140.6 7.5 %fusion.16 = f32[1024,896]{1,0:T(8,128)S(1)} fusion(bf16[1024,2048]{1,0:T(8,128)(2,1)} %bitcast.32, bf16[1,2048,896]{2,1,0:T(8,128)(2,1)} %param.28), kind=kOutput, calls=%fused_computation.26 | convolution fusion | flops 3758096384 | bytes 11534336 | tf_op jit(solution)/shard_map/dot_general | solution.py:173
  148.1 7.3 %multiply_convert_fusion = bf16[1024,896]{1,0:T(8,128)(2,1)S(1)} fusion(f32[1024,896]{1,0:T(8,128)S(1)} %fusion.16, bf16[1024,2048]{1,0:T(8,128)(2,1)} %bitcast.32, bf16[1,2048,896]{2,1,0:T(8,128)(2,1)S(1)} %copy-done.6), kind=kOutput, calls=%fused_computation.30 | convolution fusion | flops 3763601408 | bytes 13369344 | tf_op jit(solution)/shard_map/dot_general | solution.py:172
  155.5 6.1 %convolution_convert_fusion = bf16[1024,2048]{1,0:T(8,128)(2,1)} fusion(bf16[1024,896]{1,0:T(8,128)(2,1)S(1)} %multiply_convert_fusion, bf16[1,896,2048]{2,1,0:T(8,128)(2,1)S(1)} %copy-done.7), kind=kOutput, calls=%fused_computation.24 | convolution fusion | flops 3760193536 | bytes 9699328 | tf_op jit(solution)/shard_map/dot_general | solution.py:181
  161.5 5.2 %all-to-all-start.3 = ((bf16[4,256,2048]{2,1,0:T(8,128)(2,1)}), bf16[4,256,2048]{2,1,0:T(8,128)(2,1)}, u32[]{:S(2)}, u32[]{:S(2)}) async-start(bf16[4,256,2048]{2,1,0:T(8,128)(2,1)} %bitcast.122), calls=%async_computation.3 | async-start | bytes 8388608 | tf_op jit(solution)/shard_map/all_to_all | solution.py:40
  166.7 0.1 copy.80
  166.9 11.1 %copy.79 = bf16[8,4,2,192,1,128]{3,2,1,0,5,4:T(2,128)(2,1)} copy(bf16[8,4,2,192,1,128]{5,3,1,0,2,4:T(8,128)(2,1)} %bitcast.123) | data formatting | bytes 6291456 | tf_op jit(solution)/shard_map/transpose | solution.py:26
  178.0 9.8 %reshape_reshape_reshape.3 = bf16[12288,1,2,64]{0,3,2,1:T(8,128)(2,1)} reshape(bf16[8,4,2,192,1,128]{3,2,1,0,5,4:T(2,128)(2,1)} %copy.79) | data formatting | bytes 6291456 | tf_op jit(solution)/shard_map/reshape;reshape;reshape | solution.py:108
  187.9 3.9 %copy.81 = bf16[8,4,2,192,1,128]{5,3,2,1,0,4:T(8,128)(2,1)} copy(bf16[8,4,2,192,1,128]{5,3,1,0,2,4:T(8,128)(2,1)} %bitcast.125) | data formatting | bytes 6291456 | tf_op jit(solution)/shard_map/transpose | solution.py:26
  191.9 25.5 %while.17 = (s32[]{:T(128)}, f32[1,2,2,192]{3,1,2,0:T(2,128)S(1)}, f32[1,2,2,192]{3,1,2,0:T(2,128)S(1)}, f32[1,2,2,192,128]{4,3,2,1,0:T(8,128)S(1)}, s32[192]{0:...) while((s32[]{:T(128)}, f32[1,2,2,192]{3,1,2,0:T(2,128)S(1)}, ...), condition=%wide.region_5.6_spmd, body=%wide.region_0.5_spmd.sunk | while | flops 232147968 | bytes 8857645 | solution.py:128
  191.9 0.6 slice.57
  193.2 4.3 %conditional.2 = ((f32[1,2,2,192]{3,1,2,0:T(2,128)S(1)}, f32[1,2,2,192]{3,1,2,0:T(2,128)S(1)}, f32[1,2,2,192,128]{4,3,2,1,0:T(8,128)S(1)})) conditional(s32[]{:T(128)} %convert_element_type.91, (f32[1,2,2,192]{3,1,2,0:T(2,128)S(1)}, f32[1,2,2,192]{3,1,2,0:T(2,128)S(1)}, f32[1,2,2,192,128]{4,3,2,1,0:T(8,128)S(1)}) %tuple.61, (s32[]{:T(128)}, ...), branch_computations={%region_1.0_spmd, %region_2.4_spmd} | conditional | flops 232147968 | bytes 8857422 | solution.py:125
  193.2 0.1 broadcast_compare_fusion
  193.4 1.6 fusion
  195.0 0.9 fusion.4
  195.9 1.5 fusion.3
  197.5 0.6 slice.57
  198.8 0.6 slice.57
  200.1 0.6 slice.57
  201.5 0.6 slice.57
  202.8 0.6 slice.57
  204.1 0.6 slice.57
  205.4 0.6 slice.57
  206.8 0.6 slice.57
  208.1 0.6 slice.57
  209.4 0.6 slice.57
  210.7 0.6 slice.57
  212.1 0.6 slice.57
  213.4 0.6 slice.57
  214.7 0.6 slice.57
  216.0 0.6 slice.57
  217.4 0.3 multiply_reduce_fusion.1
  217.7 0.1 fusion.32
  217.9 1.3 convolution_convert_fusion.2
  219.3 4.0 %all-to-all-start = ((bf16[4,48,2048]{2,1,0:T(8,128)(2,1)}), bf16[4,48,2048]{2,1,0:T(8,128)(2,1)S(1)}, u32[]{:S(2)}, u32[]{:S(2)}) async-start(bf16[4,48,2048]{2,1,0:T(8,128)(2,1)} %bitcast.30), calls=%async_computation | async-start | bytes 1572864 | tf_op jit(solution)/shard_map/all_to_all | solution.py:40
  223.3 3.1 reduce_sum.78
  226.3 1.2 all_to_all.28
  227.6 5.9 %all-to-all-done = bf16[4,48,2048]{2,1,0:T(8,128)(2,1)S(1)} async-done(((bf16[4,48,2048]{2,1,0:T(8,128)(2,1)}), bf16[4,48,2048]{2,1,0:T(8,128)(2,1)S(1)}, u32[]{:S(2)}, u32[]{:S(2)}) %all-to-all-start) | async-done | bytes 786464 | tf_op jit(solution)/shard_map/all_to_all | solution.py:40
  233.4 0.9 copy-done.1
  234.3 72.2 %all-to-all-start.4 = ((bf16[64,4,2048]{2,1,0:T(4,128)(2,1)}), bf16[64,4,2048]{2,1,0:T(4,128)(2,1)S(1)}, u32[]{:S(2)}, u32[]{:S(2)}) async-start(bf16[64,4,2048]{2,1,0:T(4,128)(2,1)} %all_to_all.28), calls=%async_computation.4 | async-start | bytes 2097152 | tf_op jit(solution)/shard_map/all_to_all | solution.py:187
  306.7 0.1 reshape.225
  306.8 0.1 copy.90
  307.0 2.0 reduce_sum.74
  309.0 25.7 %all-to-all-done.4 = bf16[64,4,2048]{2,1,0:T(4,128)(2,1)S(1)} async-done(((bf16[64,4,2048]{2,1,0:T(4,128)(2,1)}), bf16[64,4,2048]{2,1,0:T(4,128)(2,1)S(1)}, u32[]{:S(2)}, u32[]{:S(2)}) %all-to-all-start.4) | async-done | bytes 1048608 | tf_op jit(solution)/shard_map/all_to_all | solution.py:187
  334.7 0.3 all_to_all.30
  335.0 1.1 gather_fusion
  336.1 0.5 reshape.224
  336.6 4.2 %multiply_reduce_fusion = bf16[96,2048]{1,0:T(8,128)(2,1)} fusion(bf16[96,2,2048]{2,1,0:T(2,128)(2,1)S(1)} %reshape.224, pred[96,2]{1,0:T(8,128)(4,1)S(1)} %copy.90, f32[96,2]{1,0:T(8,128)S(1)} %copy.85), kind=kLoop, calls=%fused_computation.33 | loop fusion | flops 1376256 | bytes 1180608 | tf_op jit(solution)/shard_map/reduce_sum | solution.py:189
  (68 shorter events, 1.3 us)
Async XLA Ops:
  7.2 210.8 %copy-start = (bf16[2,128,2048]{2,1,0:T(8,128)(2,1)S(1)}, bf16[2,128,2048]{2,1,0:T(8,128)(2,1)}, u32[]{:S(2)}) copy-start(bf16[2,128,2048]{2,1,0:T(8,128)(2,1)} %param.22) | copy-start | bytes 3145732
  7.2 77.8 %all-gather.7.cloned.1.call-start = ((), (), s32[]{:S(2)}) async-start(), calls=%async_computation.5 | async-start | bytes 1769472 | tf_op jit(solution)/shard_map/all_gather | solution.py:22
  19.9 88.8 %all-gather.11.cloned.1.call-start = ((), (), s32[]{:S(2)}) async-start(), calls=%async_computation.7 | async-start | bytes 1769472 | tf_op jit(solution)/shard_map/all_gather | solution.py:22
  30.1 136.7 %all-gather.9.cloned.1.call-start = ((), (), s32[]{:S(2)}) async-start(), calls=%async_computation.6 | async-start | bytes 4718592 | tf_op jit(solution)/shard_map/all_gather | solution.py:22
  87.5 53.1 %all-to-all-start.2 = ((bf16[4,256,2048]{2,1,0:T(8,128)(2,1)}), bf16[4,256,2048]{2,1,0:T(8,128)(2,1)}, u32[]{:S(2)}, u32[]{:S(2)}) async-start(bf16[4,256,2048]{2,1,0:T(8,128)(2,1)} %stack.10), calls=%async_computation.2 | async-start | bytes 8388608 | tf_op jit(solution)/shard_map/all_to_all | solution.py:170
  92.4 95.5 %all-gather.13.cloned.1.call-start = ((), (), s32[]{:S(2)}) async-start(), calls=%async_computation.8 | async-start | bytes 4718592 | tf_op jit(solution)/shard_map/all_gather | solution.py:22
  140.6 7.5 %copy-start.6 = (bf16[1,2048,896]{2,1,0:T(8,128)(2,1)S(1)}, bf16[1,2048,896]{2,1,0:T(8,128)(2,1)}, u32[]{:S(2)}) copy-start(bf16[1,2048,896]{2,1,0:T(8,128)(2,1)} %param.27) | copy-start | bytes 11010052
  148.1 7.4 %copy-start.7 = (bf16[1,896,2048]{2,1,0:T(8,128)(2,1)S(1)}, bf16[1,896,2048]{2,1,0:T(8,128)(2,1)}, u32[]{:S(2)}) copy-start(bf16[1,896,2048]{2,1,0:T(8,128)(2,1)} %param.29) | copy-start | bytes 11010052
  161.5 5.2 %copy-start.2 = (bf16[192,2,128]{2,1,0:T(2,128)(2,1)S(1)}, bf16[192,2,128]{2,1,0:T(2,128)(2,1)}, u32[]{:S(2)}) copy-start(bf16[192,2,128]{2,1,0:T(2,128)(2,1)} %param.17) | copy-start | bytes 294916
  161.5 57.7 %all-to-all-start.3 = ((bf16[4,256,2048]{2,1,0:T(8,128)(2,1)}), bf16[4,256,2048]{2,1,0:T(8,128)(2,1)}, u32[]{:S(2)}, u32[]{:S(2)}) async-start(bf16[4,256,2048]{2,1,0:T(8,128)(2,1)} %bitcast.122), calls=%async_computation.3 | async-start | bytes 8388608 | tf_op jit(solution)/shard_map/all_to_all | solution.py:40
  191.8 25.5 %copy-start.5 = (f32[2]{0:T(128)S(1)}, f32[2]{0:T(128)}, u32[]{:S(2)}) copy-start(f32[2]{0:T(128)} %param.20) | copy-start | bytes 28
  191.9 25.8 %copy-start.4 = (f32[128]{0:T(128)S(1)}, f32[128]{0:T(128)}, u32[]{:S(2)}) copy-start(f32[128]{0:T(128)} %param.21) | copy-start | bytes 1540
  219.3 14.2 %all-to-all-start = ((bf16[4,48,2048]{2,1,0:T(8,128)(2,1)}), bf16[4,48,2048]{2,1,0:T(8,128)(2,1)S(1)}, u32[]{:S(2)}, u32[]{:S(2)}) async-start(bf16[4,48,2048]{2,1,0:T(8,128)(2,1)} %bitcast.30), calls=%async_computation | async-start | bytes 1572864 | tf_op jit(solution)/shard_map/all_to_all | solution.py:40
  226.3 80.6 %copy-start.3 = (f32[96,2]{0,1:T(2,128)S(1)}, f32[96,2]{0,1:T(2,128)}, u32[]{:S(2)}) copy-start(f32[96,2]{0,1:T(2,128)} %param.26) | copy-start | bytes 2308
  233.4 0.9 copy-start.1
  234.3 100.4 %all-to-all-start.4 = ((bf16[64,4,2048]{2,1,0:T(4,128)(2,1)}), bf16[64,4,2048]{2,1,0:T(4,128)(2,1)S(1)}, u32[]{:S(2)}, u32[]{:S(2)}) async-start(bf16[64,4,2048]{2,1,0:T(4,128)(2,1)} %all_to_all.28), calls=%async_computation.4 | async-start | bytes 2097152 | tf_op jit(solution)/shard_map/all_to_all | solution.py:187
Sparse Core Ops, SparseCore 0:
  20.0 43.5 all-gather.6
  65.3 43.2 all-gather.10
  110.5 20.5 all-gather.8
  132.7 18.7 all-gather.12
